TPU v7x, 32 devices: a whole 2x2x4 slice. The times are simulated.
32 devices in a mesh: grp: 2 (over x), ra: 4 (over z), cb: 4 (over y, core).
Axes of the slice: x: 2, y: 2, z: 4, core: 2. Of those that a mesh axis runs over, the one named last changes fastest.
Arguments:
- tokens: bfloat16 [256, 4096], P('grp', 'ra'), parts along dimension 0, may hold values from -30 to 30
- in_gain: float32 [4096], P('ra'), may hold values from 0.1 to 1.9
- gate_weight: float32 [4096, 11264], P('ra', 'cb'), may hold values from -0.09375 to 0.09375
- gate_scale: float32 [11264], P('cb'), may hold values from 0.3 to 3
- up_weight: float32 [4096, 11264], P('ra', 'cb'), may hold values from -0.09375 to 0.09375
- up_scale: float32 [11264], P('cb'), may hold values from 0.3 to 3
- down_weight: float32 [11264, 4096], P('cb', 'ra'), may hold values from -0.0546875 to 0.0546875
- down_scale: float32 [4096], P('ra'), may hold values from 0.3 to 3
- out_gain: float32 [4096], P('ra'), may hold values from 0.1 to 1.9
Outputs:
- result: bfloat16 [256, 4096], P('grp', 'ra'), parts along dimension 0
There are 2 independent parts, one for each index of `grp`. A program takes and returns all parts, laid end to end along the dimension named above; an argument that names none is the same for every part. Nothing has to cross between parts.
All inputs are finite; a program needn't handle non-finite values.
Results may differ from a plain program's by a relative error of at most 0.008.
Values may be sent and summed in bfloat16 or wider, within the bound.
A program may use at most 64 MiB of HBM per device.

v0:
```python
import functools
import jax
import jax.numpy as jnp
from jax import lax
from jax.experimental import pallas as pl
from jax.experimental.pallas import tpu as pltpu
from jax.sharding import PartitionSpec as P

EPSILON = 1e-06
RESIDUAL = 0.5


def local(
    tokens, in_gain, gate_weight, gate_scale, up_weight, up_scale, down_weight, down_scale, out_gain
):
    tok_float = tokens.astype(jnp.float32)
    local_squares = jnp.sum(tok_float * tok_float, axis=1)
    scaled = (tok_float * in_gain[None, :]).astype(jnp.bfloat16)
    gate_part = jnp.dot(
        scaled, gate_weight.astype(jnp.bfloat16), preferred_element_type=jnp.float32
    )
    up_part = jnp.dot(scaled, up_weight.astype(jnp.bfloat16), preferred_element_type=jnp.float32)
    features = tokens.shape[1] * lax.axis_size("ra")
    gate_sum, up_sum, share_squares = (
        lax.psum_scatter(gate_part, "ra", scatter_dimension=0, tiled=True),
        lax.psum_scatter(up_part, "ra", scatter_dimension=0, tiled=True),
        lax.psum_scatter(local_squares, "ra", scatter_dimension=0, tiled=True),
    )
    inv_rows = lax.rsqrt(share_squares / features + EPSILON)[:, None]
    gate_share = gate_sum * inv_rows * gate_scale[None, :]
    up_share = up_sum * inv_rows * up_scale[None, :]
    hidden_share = (jax.nn.silu(gate_share) * up_share).astype(jnp.bfloat16)
    hidden = lax.all_gather(hidden_share, "ra", axis=0, tiled=True)
    down_part = jnp.dot(
        hidden, down_weight.astype(jnp.bfloat16), preferred_element_type=jnp.float32
    )
    down_full = lax.psum(down_part, "cb")
    mixed_rows = RESIDUAL * tok_float + down_full * down_scale[None, :]
    out_total = lax.psum(jnp.sum(mixed_rows * mixed_rows, axis=1), "ra")
    inv_out = lax.rsqrt(out_total / features + EPSILON)[:, None]
    return (mixed_rows * inv_out * out_gain[None, :]).astype(jnp.bfloat16)


MESH = pl.DeviceIdType.MESH
WIDTH = 256
RS_LAG = 3
AG_LAG = 5
AHEAD = 3


def kernel(
    n,
    tok_hbm, gain_hbm, gate_hbm, gscale_hbm, up_hbm, uscale_hbm, down_hbm, dscale_hbm, ogain_hbm,
    out_ref,
    tok, gain, gate, gscale, up, uscale, down, dscale, ogain,
    scaled, part, sent, got, hidden, acc, spread, sq_own, sq_got, inv, half_sent, half_got,
    y_sent, y_got, mixed, out_own, out_got,
    small_sem, gate_sem, up_sem, down_sem, rs_send, rs_recv, ag_send, ag_recv,
    sq_send, sq_recv, half_sem, y_sem, mix_sem, out_send, out_recv,
):
    chunks, half = gate.shape[0], tok.shape[0] // 2
    rows = 2 * half
    features = tok.shape[1] * n
    z, cb = lax.axis_index("ra"), lax.axis_index("cb")
    core = lax.rem(cb, 2)
    mate = cb + 1 - 2 * core
    across = lax.rem(cb + 2, 4)
    right, left = lax.rem(z + 1, n), lax.rem(z + n - 1, n)

    smalls = [
        pltpu.make_async_copy(src, dst, small_sem.at[i])
        for i, (src, dst) in enumerate([
            (tok_hbm, tok), (gain_hbm, gain), (gscale_hbm, gscale),
            (uscale_hbm, uscale), (dscale_hbm, dscale), (ogain_hbm, ogain),
        ])
    ]

    def gate_copy(j):
        cols = pl.ds(pl.multiple_of(j * WIDTH, WIDTH), WIDTH)
        return pltpu.make_async_copy(gate_hbm.at[:, cols], gate.at[j], gate_sem.at[j])

    def up_copy(j):
        cols = pl.ds(pl.multiple_of(j * WIDTH, WIDTH), WIDTH)
        return pltpu.make_async_copy(up_hbm.at[:, cols], up.at[j], up_sem.at[j])

    def down_copy(j):
        at = pl.ds(pl.multiple_of(j * WIDTH, WIDTH), WIDTH)
        return pltpu.make_async_copy(down_hbm.at[at, :], down.at[j], down_sem.at[j])

    for copy in smalls:
        copy.start()
    for j in range(min(AHEAD, chunks)):
        gate_copy(j).start()
        up_copy(j).start()

    barrier = pltpu.get_barrier_semaphore()
    for step in range(1, n):
        for who in (cb, mate):
            pl.semaphore_signal(barrier, inc=1, device_id={"ra": lax.rem(z + step, n), "cb": who}, device_id_type=MESH)
    for who in (mate, across):
        pl.semaphore_signal(barrier, inc=1, device_id={"cb": who}, device_id_type=MESH)

    for copy in smalls:
        copy.wait()
    tok_float = tok[...].astype(jnp.float32)
    scaled[...] = (tok_float * gain[...]).astype(jnp.bfloat16)
    squares = jnp.sum(tok_float * tok_float, axis=1, keepdims=True)
    spread[...] = jnp.broadcast_to(squares, (rows, 128))
    sq_own[0] = spread[...].T[:8]

    pl.semaphore_wait(barrier, 2 * (n - 1) + 2)

    def sq_copy(step, goal):
        return pltpu.make_async_remote_copy(
            sq_own.at[0], sq_got.at[step - 1], sq_send.at[goal], sq_recv.at[step - 1],
            device_id={"ra": lax.rem(z + step, n)}, device_id_type=MESH,
        )

    for goal, end in enumerate((0, n - 1)):
        for step in range(1, n):
            @pl.when(lax.rem(z + step, n) == end)
            def _():
                sq_copy(step, goal).start()

    def rs_copy(j, side):
        return pltpu.make_async_remote_copy(
            sent.at[side, j], got.at[side, j], rs_send.at[side, j], rs_recv.at[side, j],
            device_id={"ra": right if side else left}, device_id_type=MESH,
        )

    def ag_copy(j, side):
        ref = hidden.at[j, pl.ds(side * half, half)]
        return pltpu.make_async_remote_copy(
            ref, ref, ag_send.at[side, j], ag_recv.at[side, j],
            device_id={"ra": left if side else right}, device_id_type=MESH,
        )

    def rs_step(t, side):
        place = z if side else n - 1 - z
        j = t - RS_LAG * place
        own = pl.ds(side * half, half)

        @pl.when((j >= 0) & (j < chunks))
        def _():
            @pl.when(place == 0)
            def _():
                sent[side, j] = part[j, own].astype(jnp.bfloat16)
                rs_copy(j, side).start()

            @pl.when((place > 0) & (place < n - 1))
            def _():
                rs_copy(j, side).wait_recv()
                sent[side, j] = (part[j, own] + got[side, j].astype(jnp.float32)).astype(jnp.bfloat16)
                rs_copy(j, side).start()

            @pl.when(place == n - 1)
            def _():
                @pl.when(j == 0)
                def _():
                    for step in range(1, n):
                        sq_copy(step, 0).wait_recv()
                    total = sq_own[0] + sq_got[0]
                    for step in range(2, n):
                        total = total + sq_got[step - 1]
                    spread[...] = jnp.broadcast_to(total[:1], (128, 128)).T
                    inv[...] = lax.rsqrt(spread[...] / features + EPSILON)

                rs_copy(j, side).wait_recv()
                scale = inv[own]
                total = part[j, own] + got[side, j].astype(jnp.float32)
                tiles = WIDTH // 128
                for i in range(tiles):
                    at, cols = pl.ds(j * tiles + i, 1), slice(128 * i, 128 * (i + 1))
                    gate_share = total[:, cols] * scale * gscale[at]
                    up_share = total[:, WIDTH:][:, cols] * scale * uscale[at]
                    hidden[j, own, cols] = (jax.nn.silu(gate_share) * up_share).astype(jnp.bfloat16)
                ag_copy(j, side).start()

    def rs_loop(t, carry):
        @pl.when(t < chunks)
        def _():
            gate_copy(t).wait()
            part[t, :, :WIDTH] = jnp.dot(scaled[...], gate[t].astype(jnp.bfloat16), preferred_element_type=jnp.float32)
            up_copy(t).wait()

            @pl.when(t + AHEAD < chunks)
            def _():
                gate_copy(t + AHEAD).start()
                up_copy(t + AHEAD).start()

            @pl.when(t == chunks - 1)
            def _():
                for j in range(chunks):
                    down_copy(j).start()

            part[t, :, WIDTH:] = jnp.dot(scaled[...], up[t].astype(jnp.bfloat16), preferred_element_type=jnp.float32)

        rs_step(t, 0)
        rs_step(t, 1)
        return carry

    lax.fori_loop(0, chunks + RS_LAG * (n - 1), rs_loop, 0)

    def ag_step(u, side):
        place = n - 1 - z if side else z
        j = u - AG_LAG * (place - 1)

        @pl.when((place > 0) & (j >= 0) & (j < chunks))
        def _():
            ag_copy(j, side).wait_recv()

            @pl.when(place < n - 1)
            def _():
                ag_copy(j, side).start()

    acc[...] = jnp.zeros_like(acc)

    def ag_loop(u, carry):
        ag_step(u, 0)
        ag_step(u, 1)
        j = u - AG_LAG * (lax.max(z, n - 1 - z) - 1)

        @pl.when((j >= 0) & (j < chunks))
        def _():
            down_copy(j).wait()
            acc[...] += jnp.dot(hidden[j], down[j].astype(jnp.bfloat16), preferred_element_type=jnp.float32)

        return carry

    lax.fori_loop(0, chunks + AG_LAG * (n - 2), ag_loop, 0)

    mine = pl.ds(pl.multiple_of(core * half, half), half)
    theirs = pl.ds(pl.multiple_of((1 - core) * half, half), half)
    half_sent[...] = acc[theirs].astype(jnp.bfloat16)
    half_copy = pltpu.make_async_remote_copy(
        half_sent, half_got, half_sem.at[0], half_sem.at[1], device_id={"cb": mate}, device_id_type=MESH
    )
    half_copy.start()
    half_copy.wait()
    y_sent[...] = (acc[mine] + half_got[...].astype(jnp.float32)).astype(jnp.bfloat16)
    y_copy = pltpu.make_async_remote_copy(
        y_sent, y_got, y_sem.at[0], y_sem.at[1], device_id={"cb": across}, device_id_type=MESH
    )
    y_copy.start()
    y_copy.wait()
    summed = y_sent[...].astype(jnp.float32) + y_got[...].astype(jnp.float32)
    mixed[0] = RESIDUAL * tok[mine].astype(jnp.float32) + summed * dscale[...]
    mix_copy = pltpu.make_async_remote_copy(
        mixed.at[0], mixed.at[1], mix_sem.at[0], mix_sem.at[1], device_id={"cb": mate}, device_id_type=MESH
    )
    mix_copy.start()
    squares = jnp.sum(mixed[0] * mixed[0], axis=1, keepdims=True)
    spread[...] = jnp.zeros_like(spread)
    spread[mine] = jnp.broadcast_to(squares, (half, 128))
    out_own[...] = spread[...].T[:8]

    def out_copies():
        made = []
        for step in range(n):
            for other in range(2):
                if step or other:
                    at = 2 * step + other - 1
                    made.append(pltpu.make_async_remote_copy(
                        out_own, out_got.at[at], out_send.at[at], out_recv.at[at],
                        device_id={"ra": lax.rem(z + step, n), "cb": mate if other else cb},
                        device_id_type=MESH,
                    ))
        return made

    for copy in out_copies():
        copy.start()
    for copy in out_copies():
        copy.wait_recv()
    total = out_own[...]
    for at in range(2 * n - 1):
        total = total + out_got[at]
    spread[...] = jnp.broadcast_to(total[:1], (128, 128)).T
    spread[...] = lax.rsqrt(spread[...] / features + EPSILON)
    out_ref[mine] = (mixed[0] * spread[mine][:, :1] * ogain[...]).astype(jnp.bfloat16)
    mix_copy.wait()
    out_ref[theirs] = (mixed[1] * spread[theirs][:, :1] * ogain[...]).astype(jnp.bfloat16)

    for copy in out_copies():
        copy.wait_send()
    for goal, end in enumerate((0, n - 1)):
        @pl.when(z != end)
        def _():
            sq_copy(1, goal).wait_send()

    def drain(j, carry):
        @pl.when(z > 0)
        def _():
            rs_copy(j, 0).wait_send()
            ag_copy(j, 1).wait_send()

        @pl.when(z < n - 1)
        def _():
            rs_copy(j, 1).wait_send()
            ag_copy(j, 0).wait_send()

        return carry

    lax.fori_loop(0, chunks, drain, 0)


def fused(
    tokens, in_gain, gate_weight, gate_scale, up_weight, up_scale, down_weight, down_scale, out_gain
):
    n = lax.axis_size("ra")
    rows, depth = tokens.shape
    units, width = down_weight.shape
    half, chunks = rows // 2, units // WIDTH
    f32, bf16 = jnp.float32, jnp.bfloat16
    vmem, dma = pltpu.VMEM, pltpu.SemaphoreType.DMA
    return pl.pallas_call(
        functools.partial(kernel, n),
        out_shape=jax.ShapeDtypeStruct((rows, width), bf16),
        in_specs=[pl.BlockSpec(memory_space=pl.ANY)] * 9,
        out_specs=pl.BlockSpec(memory_space=pltpu.VMEM),
        scratch_shapes=[
            vmem((rows, depth), bf16), vmem((1, depth), f32),
            vmem((chunks, depth, WIDTH), f32), vmem((units // 128, 128), f32),
            vmem((chunks, depth, WIDTH), f32), vmem((units // 128, 128), f32),
            vmem((chunks, WIDTH, width), f32), vmem((1, width), f32), vmem((1, width), f32),
            vmem((rows, depth), bf16), vmem((chunks, rows, 2 * WIDTH), f32),
            vmem((2, chunks, half, 2 * WIDTH), bf16), vmem((2, chunks, half, 2 * WIDTH), bf16),
            vmem((chunks, rows, WIDTH), bf16), vmem((rows, width), f32),
            vmem((rows, 128), f32), vmem((1, 8, 128), f32), vmem((n - 1, 8, 128), f32),
            vmem((rows, 128), f32), vmem((half, width), bf16), vmem((half, width), bf16),
            vmem((half, width), bf16), vmem((half, width), bf16), vmem((2, half, width), f32),
            vmem((8, 128), f32), vmem((2 * n - 1, 8, 128), f32),
            dma((6,)), dma((chunks,)), dma((chunks,)), dma((chunks,)),
            dma((2, chunks)), dma((2, chunks)), dma((2, chunks)), dma((2, chunks)),
            dma((2,)), dma((n - 1,)), dma((2,)), dma((2,)), dma((2,)),
            dma((2 * n - 1,)), dma((2 * n - 1,)),
        ],
        compiler_params=pltpu.CompilerParams(
            collective_id=0, has_side_effects=True, vmem_limit_bytes=60 * 2**20
        ),
        name="fused_ffn",
    )(
        tokens, in_gain.reshape(1, -1), gate_weight, gate_scale.reshape(-1, 128), up_weight,
        up_scale.reshape(-1, 128), down_weight, down_scale.reshape(1, -1), out_gain.reshape(1, -1),
    )


def solution(mesh):
    in_specs = (
        P("grp", "ra"),
        P("ra"),
        P("ra", "cb"),
        P("cb"),
        P("ra", "cb"),
        P("cb"),
        P("cb", "ra"),
        P("ra"),
        P("ra"),
    )
    out_specs = P("grp", "ra")
    body = fused if mesh.shape["ra"] == 4 and mesh.shape["cb"] == 4 else local
    return jax.shard_map(body, mesh=mesh, in_specs=in_specs, out_specs=out_specs, check_vma=False)
```

profile of v0, /device:TPU:0, one launch (start us, length us, event | category | flops | bytes accessed | tf_op | source)
XLA Modules:
  0.0 55.1 jit_solution(12540979206602697261)
XLA Ops:
  0.0 53.5 %fused_ffn.1 = bf16[128,1024]{1,0:T(8,128)(2,1)} custom-call(bf16[128,1024]{1,0:T(8,128)(2,1)} %tok_hbm.1, f32[1,1024]{1,0:T(1,128)} %bitcast.7, f32[1024,2816]{1,0:T(8,128)} %gate_hbm.1, f32[22,128]{1,0:T(8,128)} %bitcast.5, f32[1024,2816]{1,0:T(8,128)} %up_hbm.1, f32[22,128]{1,0:T(8,128)} %bitcast.6, f32[2816,1024]{1,0:T(8,128)} %down_hbm.1, ...), custom_call_target="tpu_custom_call" | custom-call | tf_op jit(solution)/shard_map/fused_ffn/pallas_call | solution.py:315
  53.5 1.7 %copy.11 = bf16[128,1024]{1,0:T(8,128)(2,1)} copy(bf16[128,1024]{1,0:T(8,128)(2,1)} %fused_ffn.1) | data formatting | bytes 524288
where the time goes:
time: 55.3 us; the launch traced here: 55.1 us
  Pallas kernels  53.5 us (97%)
  local copies, waits for them, and re-layouts  1.67 us (3%)
    pallas_call x1, Pallas kernels, fused(): pl.pallas_call(functools.partial(kernel, n), out_shape=jax.ShapeDtypeStru...  53.5 us
    unnamed x1, local copies, waits for them, and re-layouts  1.67 us

commit v1 on v0

v1 whole, which is shorter than its diff:
```python
import functools
import jax
import jax.numpy as jnp
from jax import lax
from jax.experimental import pallas as pl
from jax.experimental.pallas import tpu as pltpu
from jax.sharding import PartitionSpec as P

EPSILON = 1e-06
RESIDUAL = 0.5


def local(
    tokens, in_gain, gate_weight, gate_scale, up_weight, up_scale, down_weight, down_scale, out_gain
):
    tok_float = tokens.astype(jnp.float32)
    local_squares = jnp.sum(tok_float * tok_float, axis=1)
    scaled = (tok_float * in_gain[None, :]).astype(jnp.bfloat16)
    gate_part = jnp.dot(
        scaled, gate_weight.astype(jnp.bfloat16), preferred_element_type=jnp.float32
    )
    up_part = jnp.dot(scaled, up_weight.astype(jnp.bfloat16), preferred_element_type=jnp.float32)
    features = tokens.shape[1] * lax.axis_size("ra")
    gate_sum, up_sum, share_squares = (
        lax.psum_scatter(gate_part, "ra", scatter_dimension=0, tiled=True),
        lax.psum_scatter(up_part, "ra", scatter_dimension=0, tiled=True),
        lax.psum_scatter(local_squares, "ra", scatter_dimension=0, tiled=True),
    )
    inv_rows = lax.rsqrt(share_squares / features + EPSILON)[:, None]
    gate_share = gate_sum * inv_rows * gate_scale[None, :]
    up_share = up_sum * inv_rows * up_scale[None, :]
    hidden_share = (jax.nn.silu(gate_share) * up_share).astype(jnp.bfloat16)
    hidden = lax.all_gather(hidden_share, "ra", axis=0, tiled=True)
    down_part = jnp.dot(
        hidden, down_weight.astype(jnp.bfloat16), preferred_element_type=jnp.float32
    )
    down_full = lax.psum(down_part, "cb")
    mixed_rows = RESIDUAL * tok_float + down_full * down_scale[None, :]
    out_total = lax.psum(jnp.sum(mixed_rows * mixed_rows, axis=1), "ra")
    inv_out = lax.rsqrt(out_total / features + EPSILON)[:, None]
    return (mixed_rows * inv_out * out_gain[None, :]).astype(jnp.bfloat16)


MESH = pl.DeviceIdType.MESH
WIDTH = 256
SUB = 128
AHEAD = 3
RS_LAG = ((22, 8, 4, 0), (0, 3, 7, 22))
AG_LAG = ((0, 25, 32, 44), (44, 32, 29, 0))
OWN_SEND = (45, 37, 41, 45)
OWN_PASS = (47, 39, 43, 47)
STEPS = 56


def pick(z, values):
    out = jnp.int32(values[0])
    for i, value in enumerate(values[1:], 1):
        out = lax.select(z == i, jnp.int32(value), out)
    return out


def kernel(
    n,
    tok_hbm, gain_hbm, gate_hbm, gscale_hbm, up_hbm, uscale_hbm, down_hbm, dscale_hbm, ogain_hbm,
    out_ref,
    tok, gain, gate, gscale, up, uscale, down, dscale, ogain,
    scaled, part, sent, got, hidden, acc, spread, sq_own, sq_sent, sq_got, inv,
    mate_sent, mate_got, y_sent, y_got, mixed, mixed_got, out_all,
    small_sem, gate_sem, up_sem, down_sem, rs_send, rs_recv, ag_send, ag_recv,
    sq_send, sq_recv, mate_sem, y_sem, mix_sem, out_send, out_recv,
):
    blocks, half = gate.shape[0], tok.shape[0] // 2
    chunks = part.shape[0]
    per = chunks // blocks
    rows = 2 * half
    wide = tok.shape[1] // 2
    features = tok.shape[1] * n
    z, cb = lax.axis_index("ra"), lax.axis_index("cb")
    core = lax.rem(cb, 2)
    mate = cb + 1 - 2 * core
    across = lax.rem(cb + 2, 4)
    right, left = lax.rem(z + 1, n), lax.rem(z + n - 1, n)
    own_side = (z >= n // 2).astype(jnp.int32)
    mine = pl.ds(pl.multiple_of(core * wide, wide), wide)
    theirs = pl.ds(pl.multiple_of((1 - core) * wide, wide), wide)

    smalls = [
        pltpu.make_async_copy(src, dst, small_sem.at[i])
        for i, (src, dst) in enumerate([
            (tok_hbm, tok), (gain_hbm, gain), (gscale_hbm, gscale),
            (uscale_hbm, uscale), (dscale_hbm, dscale), (ogain_hbm, ogain),
        ])
    ]

    def gate_copy(k):
        cols = pl.ds(pl.multiple_of(k * WIDTH, WIDTH), WIDTH)
        return pltpu.make_async_copy(gate_hbm.at[:, cols], gate.at[k], gate_sem.at[k])

    def up_copy(k):
        cols = pl.ds(pl.multiple_of(k * WIDTH, WIDTH), WIDTH)
        return pltpu.make_async_copy(up_hbm.at[:, cols], up.at[k], up_sem.at[k])

    def down_copy(k):
        at = pl.ds(pl.multiple_of(k * WIDTH, WIDTH), WIDTH)
        return pltpu.make_async_copy(down_hbm.at[at, :], down.at[k], down_sem.at[k])

    for copy in smalls[:2]:
        copy.start()
    for k in range(min(AHEAD, blocks)):
        gate_copy(k).start()
        up_copy(k).start()
    for copy in smalls[2:]:
        copy.start()

    barrier = pltpu.get_barrier_semaphore()

    @pl.when(z > 0)
    def _():
        pl.semaphore_signal(barrier, inc=1, device_id={"ra": left}, device_id_type=MESH)

    @pl.when(z < n - 1)
    def _():
        pl.semaphore_signal(barrier, inc=1, device_id={"ra": right}, device_id_type=MESH)

    for who in (mate, across):
        pl.semaphore_signal(barrier, inc=1, device_id={"cb": who}, device_id_type=MESH)

    for copy in smalls[:2]:
        copy.wait()
    tok_float = tok[...].astype(jnp.float32)
    scaled[...] = (tok_float * gain[...]).astype(jnp.bfloat16)
    def sq_copy(side):
        return pltpu.make_async_remote_copy(
            sq_sent.at[side], sq_got.at[side], sq_send.at[side], sq_recv.at[side],
            device_id={"ra": right if side else left}, device_id_type=MESH,
        )

    def rs_copy(j, side):
        return pltpu.make_async_remote_copy(
            sent.at[side, j], got.at[side, j], rs_send.at[side, j], rs_recv.at[side, j],
            device_id={"ra": right if side else left}, device_id_type=MESH,
        )

    def ag_copy(j, side):
        ref = hidden.at[side, j]
        return pltpu.make_async_remote_copy(
            ref, ref, ag_send.at[side, j], ag_recv.at[side, j],
            device_id={"ra": left if side else right}, device_id_type=MESH,
        )

    def rows_of(side):
        return pl.ds(side * half, half)

    def rs_step(s, side):
        place = z if side else n - 1 - z
        j = s - pick(z, RS_LAG[side])

        @pl.when((j >= 0) & (j < chunks) & (place > 0))
        def _():
            @pl.when(place < n - 1)
            def _():
                @pl.when(j == 0)
                def _():
                    sq_copy(side).wait_recv()
                    sq_sent[side] = sq_own[...] + sq_got[side]
                    sq_copy(side).start()

                rs_copy(j, side).wait_recv()
                sent[side, j] = (part[j, rows_of(side)] + got[side, j].astype(jnp.float32)).astype(jnp.bfloat16)
                rs_copy(j, side).start()

            @pl.when(place == n - 1)
            def _():
                @pl.when(j == 0)
                def _():
                    sq_copy(side).wait_recv()
                    total = sq_own[...] + sq_got[side]
                    spread[...] = jnp.broadcast_to(total[:1], (128, 128)).T
                    inv[...] = lax.rsqrt(spread[...] / features + EPSILON)

                rs_copy(j, side).wait_recv()
                scale = inv[rows_of(side)]
                total = part[j, rows_of(side)] + got[side, j].astype(jnp.float32)
                gate_share = total[:, :SUB] * scale * gscale[pl.ds(j, 1)]
                up_share = total[:, SUB:] * scale * uscale[pl.ds(j, 1)]
                hidden[side, j] = (jax.nn.silu(gate_share) * up_share).astype(jnp.bfloat16)
                ag_copy(j, side).start()

    def ag_step(s, side, i):
        place = n - 1 - z if side else z
        j = per * (s - pick(z, AG_LAG[side])) + i

        @pl.when((j >= 0) & (j < chunks) & (place > 0))
        def _():
            ag_copy(j, side).wait_recv()

            @pl.when(place < n - 1)
            def _():
                ag_copy(j, side).start()

    def down_step(s, side):
        place = n - 1 - z if side else z
        since = s - pick(z, RS_LAG[side])
        k = lax.select(place > 0, s - pick(z, AG_LAG[side]), since // per)

        @pl.when((k >= 0) & (k < blocks) & ((place > 0) | (lax.rem(since, per) == per - 1)))
        def _():
            @pl.when(own_side == side)
            def _():
                down_copy(k).wait()

            units = jnp.concatenate([hidden[side, per * k + i] for i in range(per)], axis=1)
            weights = down[k].astype(jnp.bfloat16)
            acc[side] += jnp.dot(units, weights, preferred_element_type=jnp.float32)

    def mate_copy(side):
        return pltpu.make_async_remote_copy(
            mate_sent.at[side], mate_got.at[side], mate_sem.at[0, side], mate_sem.at[1, side],
            device_id={"cb": mate}, device_id_type=MESH,
        )

    def y_copy(side):
        return pltpu.make_async_remote_copy(
            y_sent.at[side], y_got.at[side], y_sem.at[0, side], y_sem.at[1, side],
            device_id={"cb": across}, device_id_type=MESH,
        )

    def mix_copy(side):
        at = rows_of(side)
        return pltpu.make_async_remote_copy(
            mixed.at[at], mixed_got.at[at], mix_sem.at[0, side], mix_sem.at[1, side],
            device_id={"cb": mate}, device_id_type=MESH,
        )

    def mate_start(side):
        mate_sent[side] = acc[side, :, theirs].astype(jnp.bfloat16)
        mate_copy(side).start()

    def y_start(side):
        mate_copy(side).wait_recv()
        y_sent[side] = (acc[side, :, mine] + mate_got[side].astype(jnp.float32)).astype(jnp.bfloat16)
        y_copy(side).start()

    def mix_start(side):
        y_copy(side).wait_recv()
        at = rows_of(side)
        summed = y_sent[side].astype(jnp.float32) + y_got[side].astype(jnp.float32)
        value = RESIDUAL * tok[at, mine].astype(jnp.float32) + summed * dscale[:, mine]
        mixed[at] = value
        spread[at] = jnp.broadcast_to(jnp.sum(value * value, axis=1, keepdims=True), (half, 128))

    def step(s, carry):
        @pl.when((s < chunks) & (lax.rem(s, per) == 0))
        def _():
            k = s // per

            def store(product, offset):
                for i in range(per):
                    part[s + i, :, offset:offset + SUB] = product[:, SUB * i:SUB * (i + 1)]

            gate_copy(k).wait()
            store(jnp.dot(scaled[...], gate[k].astype(jnp.bfloat16), preferred_element_type=jnp.float32), 0)
            up_copy(k).wait()

            @pl.when(k + AHEAD < blocks)
            def _():
                gate_copy(k + AHEAD).start()
                up_copy(k + AHEAD).start()

            down_copy(k).start()
            store(jnp.dot(scaled[...], up[k].astype(jnp.bfloat16), preferred_element_type=jnp.float32), SUB)
            @pl.when(k == 0)
            def _():
                tok_float = tok[...].astype(jnp.float32)
                squares = jnp.sum(tok_float * tok_float, axis=1, keepdims=True)
                spread[...] = jnp.broadcast_to(squares, (rows, 128))
                sq_own[...] = spread[...].T[:8]
                pl.semaphore_wait(barrier, 2 + (z > 0).astype(jnp.int32) + (z < n - 1).astype(jnp.int32))

            for side in range(2):
                @pl.when(z == (0 if side else n - 1))
                def _():
                    for i in range(per):
                        sent[side, s + i] = part[s + i, rows_of(side)].astype(jnp.bfloat16)
                        rs_copy(s + i, side).start()

                    @pl.when(k == 0)
                    def _():
                        sq_sent[side] = sq_own[...]
                        sq_copy(side).start()

        @pl.when(s == 0)
        def _():
            for copy in smalls[2:]:
                copy.wait()
            for side in range(2):
                acc[side] = jnp.zeros_like(acc[side])

        for side in (1, 0):
            rs_step(s, side)
        for i in range(per):
            for side in range(2):
                ag_step(s, side, i)
        for side in range(2):
            down_step(s, side)
        for side in range(2):
            @pl.when(own_side == side)
            def _():
                @pl.when(s == pick(z, OWN_SEND))
                def _():
                    mate_start(side)

                @pl.when(s == pick(z, OWN_PASS))
                def _():
                    y_start(side)

        return carry

    lax.fori_loop(0, STEPS, step, 0)

    for side in range(2):
        @pl.when(own_side != side)
        def _():
            mate_start(side)
            mix_start(1 - side)
            mix_copy(1 - side).start()
            y_start(side)
            mix_start(side)

    at = 2 * z + core
    out_all[at] = spread[...].T[:8]

    def out_copies(arriving):
        made = []
        for step in range(n):
            for other in range(2):
                if step or other:
                    slot = 2 * step + other - 1
                    source = 2 * lax.rem(z + n - step, n) + (1 - core if other else core)
                    ref = out_all.at[source if arriving else at]
                    made.append(pltpu.make_async_remote_copy(
                        ref, ref, out_send.at[slot], out_recv.at[slot],
                        device_id={"ra": lax.rem(z + step, n), "cb": mate if other else cb},
                        device_id_type=MESH,
                    ))
        return made

    for copy in out_copies(False):
        copy.start()
    for side in range(2):
        @pl.when(own_side != side)
        def _():
            mix_copy(side).start()

    for side in range(2):
        mate_copy(side).wait_send()
        y_copy(side).wait_send()

        @pl.when(z != (n - 1 if side else 0))
        def _():
            sq_copy(side).wait_send()

    def drain(j, carry):
        @pl.when(z > 0)
        def _():
            rs_copy(j, 0).wait_send()
            ag_copy(j, 1).wait_send()

        @pl.when(z < n - 1)
        def _():
            rs_copy(j, 1).wait_send()
            ag_copy(j, 0).wait_send()

        return carry

    lax.fori_loop(0, chunks, drain, 0)

    for copy in out_copies(True):
        copy.wait_recv()
    total = out_all[0]
    for i in range(1, 2 * n):
        total = total + out_all[i]
    spread[...] = jnp.broadcast_to(total[:1], (128, 128)).T
    spread[...] = lax.rsqrt(spread[...] / features + EPSILON)
    out_ref[:, mine] = (mixed[...] * spread[:, :1] * ogain[:, mine]).astype(jnp.bfloat16)
    for side in range(2):
        mix_copy(side).wait_recv()
    out_ref[:, theirs] = (mixed_got[...] * spread[:, :1] * ogain[:, theirs]).astype(jnp.bfloat16)
    for side in range(2):
        mix_copy(side).wait_send()
    for copy in out_copies(False):
        copy.wait_send()


def fused(
    tokens, in_gain, gate_weight, gate_scale, up_weight, up_scale, down_weight, down_scale, out_gain
):
    n = lax.axis_size("ra")
    rows, depth = tokens.shape
    units, width = down_weight.shape
    half, blocks, chunks = rows // 2, units // WIDTH, units // SUB
    wide = width // 2
    f32, bf16 = jnp.float32, jnp.bfloat16
    vmem, dma = pltpu.VMEM, pltpu.SemaphoreType.DMA
    return pl.pallas_call(
        functools.partial(kernel, n),
        out_shape=pltpu.VMEM((rows, width), bf16),
        in_specs=[pl.BlockSpec(memory_space=pltpu.HBM)] * 9,
        out_specs=pl.BlockSpec(memory_space=pltpu.VMEM),
        scratch_shapes=[
            vmem((rows, depth), bf16), vmem((1, depth), f32),
            vmem((blocks, depth, WIDTH), f32), vmem((units // 128, 128), f32),
            vmem((blocks, depth, WIDTH), f32), vmem((units // 128, 128), f32),
            vmem((blocks, WIDTH, width), f32), vmem((1, width), f32), vmem((1, width), f32),
            vmem((rows, depth), bf16), vmem((chunks, rows, 2 * SUB), f32),
            vmem((2, chunks, half, 2 * SUB), bf16), vmem((2, chunks, half, 2 * SUB), bf16),
            vmem((2, chunks, half, SUB), bf16), vmem((2, half, width), f32),
            vmem((rows, 128), f32), vmem((8, 128), f32), vmem((2, 8, 128), f32), vmem((2, 8, 128), f32),
            vmem((rows, 128), f32),
            vmem((2, half, wide), bf16), vmem((2, half, wide), bf16),
            vmem((2, half, wide), bf16), vmem((2, half, wide), bf16),
            vmem((rows, wide), f32), vmem((rows, wide), f32), vmem((2 * n, 8, 128), f32),
            dma((6,)), dma((blocks,)), dma((blocks,)), dma((blocks,)),
            dma((2, chunks)), dma((2, chunks)), dma((2, chunks)), dma((2, chunks)),
            dma((2,)), dma((2,)), dma((2, 2)), dma((2, 2)), dma((2, 2)),
            dma((2 * n - 1,)), dma((2 * n - 1,)),
        ],
        compiler_params=pltpu.CompilerParams(
            collective_id=0, has_side_effects=True, vmem_limit_bytes=60 * 2**20
        ),
        name="fused_ffn",
    )(
        tokens, in_gain.reshape(1, -1), gate_weight, gate_scale.reshape(-1, 128), up_weight,
        up_scale.reshape(-1, 128), down_weight, down_scale.reshape(1, -1), out_gain.reshape(1, -1),
    )


def solution(mesh):
    in_specs = (
        P("grp", "ra"),
        P("ra"),
        P("ra", "cb"),
        P("cb"),
        P("ra", "cb"),
        P("cb"),
        P("cb", "ra"),
        P("ra"),
        P("ra"),
    )
    out_specs = P("grp", "ra")
    body = fused if mesh.shape["ra"] == 4 and mesh.shape["cb"] == 4 else local
    return jax.shard_map(body, mesh=mesh, in_specs=in_specs, out_specs=out_specs, check_vma=False)
```

time: 55.3 us -> 50.3 us (0.910)
  Pallas kernels: 53.5 us -> 49.4 us
  local copies, waits for them, and re-layouts: 1.67 us -> 0.71 us
    pallas_call x1, Pallas kernels: 53.5 us -> 49.4 us  [fused(): pl.pallas_call(functools.partial(kernel, n), out_shape=pltpu.VMEM((rows,...]
    unnamed x1, local copies, waits for them, and re-layouts: 1.67 us -> 0.71 us
where the time goes in v1:
time: 50.3 us; the launch traced here: 50.1 us
  Pallas kernels  49.4 us (98%)
  local copies, waits for them, and re-layouts  0.71 us (1%)
    pallas_call x1, Pallas kernels, fused(): pl.pallas_call(functools.partial(kernel, n), out_shape=pltpu.VMEM((rows,...  49.4 us

profile of v1, /device:TPU:0, one launch (start us, length us, event | category | flops | bytes accessed | tf_op | source)
XLA Modules:
  0.0 50.1 jit_solution(15867865704072174255)
XLA Ops:
  0.0 49.4 %fused_ffn.1 = bf16[128,1024]{1,0:T(8,128)(2,1)S(1)} custom-call(bf16[128,1024]{1,0:T(8,128)(2,1)} %tok_hbm.1, f32[1,1024]{1,0:T(1,128)} %bitcast.7, f32[1024,2816]{1,0:T(8,128)} %gate_hbm.1, f32[22,128]{1,0:T(8,128)} %bitcast.5, f32[1024,2816]{1,0:T(8,128)} %up_hbm.1, f32[22,128]{1,0:T(8,128)} %bitcast.6, f32[2816,1024]{1,0:T(8,128)} %down_hbm.1, ...), custom_call_target="tpu_custom_call" | custom-call | tf_op jit(solution)/shard_map/fused_ffn/pallas_call | solution.py:405
  49.4 0.7 %copy.11 = bf16[128,1024]{1,0:T(8,128)(2,1)} copy(bf16[128,1024]{1,0:T(8,128)(2,1)S(1)} %fused_ffn.1) | data formatting | bytes 524288

commit v2 on v1

--- a/solution.py
+++ b/solution.py
@@ -44,11 +44,12 @@
 MESH = pl.DeviceIdType.MESH
 WIDTH = 256
 SUB = 128
-AHEAD = 3
-RS_LAG = ((22, 8, 4, 0), (0, 3, 7, 22))
-AG_LAG = ((0, 25, 32, 44), (44, 32, 29, 0))
-OWN_SEND = (45, 37, 41, 45)
-OWN_PASS = (47, 39, 43, 47)
+AHEAD = 6
+DOWN_START = 17
+RS_LAG = ((22, 12, 9, 0), (0, 7, 12, 22))
+AG_LAG = ((0, 28, 34, 44), (44, 34, 30, 0))
+OWN_SEND = (45, 40, 42, 45)
+OWN_PASS = (47, 42, 44, 47)
 STEPS = 56
 
 
@@ -67,9 +68,9 @@
     scaled, part, sent, got, hidden, acc, spread, sq_own, sq_sent, sq_got, inv,
     mate_sent, mate_got, y_sent, y_got, mixed, mixed_got, out_all,
     small_sem, gate_sem, up_sem, down_sem, rs_send, rs_recv, ag_send, ag_recv,
-    sq_send, sq_recv, mate_sem, y_sem, mix_sem, out_send, out_recv,
+    sq_send, sq_recv, mate_sem, y_sem, mix_sem, out_sem,
 ):
-    blocks, half = gate.shape[0], tok.shape[0] // 2
+    blocks, half = down.shape[0] // WIDTH, tok.shape[0] // 2
     chunks = part.shape[0]
     per = chunks // blocks
     rows = 2 * half
@@ -92,25 +93,20 @@
         ])
     ]
 
-    def gate_copy(k):
-        cols = pl.ds(pl.multiple_of(k * WIDTH, WIDTH), WIDTH)
-        return pltpu.make_async_copy(gate_hbm.at[:, cols], gate.at[k], gate_sem.at[k])
-
-    def up_copy(k):
-        cols = pl.ds(pl.multiple_of(k * WIDTH, WIDTH), WIDTH)
-        return pltpu.make_async_copy(up_hbm.at[:, cols], up.at[k], up_sem.at[k])
-
-    def down_copy(k):
-        at = pl.ds(pl.multiple_of(k * WIDTH, WIDTH), WIDTH)
-        return pltpu.make_async_copy(down_hbm.at[at, :], down.at[k], down_sem.at[k])
+    def gate_copy(j):
+        cols = pl.ds(pl.multiple_of(j * SUB, SUB), SUB)
+        return pltpu.make_async_copy(gate_hbm.at[:, cols], gate.at[j], gate_sem.at[lax.rem(j, AHEAD)])
+
+    def up_copy(j):
+        cols = pl.ds(pl.multiple_of(j * SUB, SUB), SUB)
+        return pltpu.make_async_copy(up_hbm.at[:, cols], up.at[j], up_sem.at[lax.rem(j, AHEAD)])
+
+    down_copy = pltpu.make_async_copy(down_hbm, down, down_sem)
 
     for copy in smalls[:2]:
         copy.start()
-    for k in range(min(AHEAD, blocks)):
-        gate_copy(k).start()
-        up_copy(k).start()
-    for copy in smalls[2:]:
-        copy.start()
+    gate_copy(0).start()
+    up_copy(0).start()
 
     barrier = pltpu.get_barrier_semaphore()
 
@@ -127,6 +123,11 @@
 
     for copy in smalls[:2]:
         copy.wait()
+    for j in range(1, min(AHEAD, chunks)):
+        gate_copy(j).start()
+        up_copy(j).start()
+    for copy in smalls[2:]:
+        copy.start()
     tok_float = tok[...].astype(jnp.float32)
     scaled[...] = (tok_float * gain[...]).astype(jnp.bfloat16)
     def sq_copy(side):
@@ -137,14 +138,14 @@
 
     def rs_copy(j, side):
         return pltpu.make_async_remote_copy(
-            sent.at[side, j], got.at[side, j], rs_send.at[side, j], rs_recv.at[side, j],
+            sent.at[side, j], got.at[side, j], rs_send.at[side], rs_recv.at[side, j],
             device_id={"ra": right if side else left}, device_id_type=MESH,
         )
 
     def ag_copy(j, side):
         ref = hidden.at[side, j]
         return pltpu.make_async_remote_copy(
-            ref, ref, ag_send.at[side, j], ag_recv.at[side, j],
+            ref, ref, ag_send.at[side], ag_recv.at[side, j],
             device_id={"ra": left if side else right}, device_id_type=MESH,
         )
 
@@ -159,18 +160,20 @@
         def _():
             @pl.when(place < n - 1)
             def _():
+                rs_copy(j, side).wait_recv()
+                sent[side, j] = (part[j, rows_of(side)] + got[side, j].astype(jnp.float32)).astype(jnp.bfloat16)
+                rs_copy(j, side).start()
+
                 @pl.when(j == 0)
                 def _():
                     sq_copy(side).wait_recv()
                     sq_sent[side] = sq_own[...] + sq_got[side]
                     sq_copy(side).start()
 
-                rs_copy(j, side).wait_recv()
-                sent[side, j] = (part[j, rows_of(side)] + got[side, j].astype(jnp.float32)).astype(jnp.bfloat16)
-                rs_copy(j, side).start()
-
             @pl.when(place == n - 1)
             def _():
+                rs_copy(j, side).wait_recv()
+
                 @pl.when(j == 0)
                 def _():
                     sq_copy(side).wait_recv()
@@ -178,7 +181,6 @@
                     spread[...] = jnp.broadcast_to(total[:1], (128, 128)).T
                     inv[...] = lax.rsqrt(spread[...] / features + EPSILON)
 
-                rs_copy(j, side).wait_recv()
                 scale = inv[rows_of(side)]
                 total = part[j, rows_of(side)] + got[side, j].astype(jnp.float32)
                 gate_share = total[:, :SUB] * scale * gscale[pl.ds(j, 1)]
@@ -205,12 +207,8 @@
 
         @pl.when((k >= 0) & (k < blocks) & ((place > 0) | (lax.rem(since, per) == per - 1)))
         def _():
-            @pl.when(own_side == side)
-            def _():
-                down_copy(k).wait()
-
             units = jnp.concatenate([hidden[side, per * k + i] for i in range(per)], axis=1)
-            weights = down[k].astype(jnp.bfloat16)
+            weights = down[pl.ds(pl.multiple_of(k * WIDTH, WIDTH), WIDTH)].astype(jnp.bfloat16)
             acc[side] += jnp.dot(units, weights, preferred_element_type=jnp.float32)
 
     def mate_copy(side):
@@ -249,55 +247,63 @@
         mixed[at] = value
         spread[at] = jnp.broadcast_to(jnp.sum(value * value, axis=1, keepdims=True), (half, 128))
 
-    def step(s, carry):
-        @pl.when((s < chunks) & (lax.rem(s, per) == 0))
-        def _():
-            k = s // per
-
-            def store(product, offset):
-                for i in range(per):
-                    part[s + i, :, offset:offset + SUB] = product[:, SUB * i:SUB * (i + 1)]
-
-            gate_copy(k).wait()
-            store(jnp.dot(scaled[...], gate[k].astype(jnp.bfloat16), preferred_element_type=jnp.float32), 0)
-            up_copy(k).wait()
-
-            @pl.when(k + AHEAD < blocks)
-            def _():
-                gate_copy(k + AHEAD).start()
-                up_copy(k + AHEAD).start()
-
-            down_copy(k).start()
-            store(jnp.dot(scaled[...], up[k].astype(jnp.bfloat16), preferred_element_type=jnp.float32), SUB)
-            @pl.when(k == 0)
-            def _():
-                tok_float = tok[...].astype(jnp.float32)
-                squares = jnp.sum(tok_float * tok_float, axis=1, keepdims=True)
-                spread[...] = jnp.broadcast_to(squares, (rows, 128))
-                sq_own[...] = spread[...].T[:8]
-                pl.semaphore_wait(barrier, 2 + (z > 0).astype(jnp.int32) + (z < n - 1).astype(jnp.int32))
-
-            for side in range(2):
-                @pl.when(z == (0 if side else n - 1))
-                def _():
-                    for i in range(per):
-                        sent[side, s + i] = part[s + i, rows_of(side)].astype(jnp.bfloat16)
-                        rs_copy(s + i, side).start()
-
-                    @pl.when(k == 0)
-                    def _():
-                        sq_sent[side] = sq_own[...]
-                        sq_copy(side).start()
-
-        @pl.when(s == 0)
-        def _():
-            for copy in smalls[2:]:
-                copy.wait()
-            for side in range(2):
-                acc[side] = jnp.zeros_like(acc[side])
-
+    def first(side):
+        return z == (0 if side else n - 1)
+
+    def dot_step(j):
+        gate_copy(j).wait()
+        up_copy(j).wait()
+        weights = jnp.concatenate([gate[j], up[j]], axis=1).astype(jnp.bfloat16)
+        part[j] = jnp.dot(scaled[...], weights, preferred_element_type=jnp.float32)
+
+    def send_step(j, side):
+        @pl.when(first(side))
+        def _():
+            sent[side, j] = part[j, rows_of(side)].astype(jnp.bfloat16)
+            rs_copy(j, side).start()
+
+    dot_step(0)
+    pl.semaphore_wait(barrier, 2 + (z > 0).astype(jnp.int32) + (z < n - 1).astype(jnp.int32))
+    for side in range(2):
+        send_step(0, side)
+    tok_float = tok[...].astype(jnp.float32)
+    squares = jnp.sum(tok_float * tok_float, axis=1, keepdims=True)
+    spread[...] = jnp.broadcast_to(squares, (rows, 128))
+    sq_own[...] = spread[...].T[:8]
+    for side in range(2):
+        @pl.when(first(side))
+        def _():
+            sq_sent[side] = sq_own[...]
+            sq_copy(side).start()
+
+    gate_copy(AHEAD).start()
+    up_copy(AHEAD).start()
+
+    def dots(s, carry):
         for side in (1, 0):
             rs_step(s, side)
+        dot_step(s)
+        for side in range(2):
+            send_step(s, side)
+
+        @pl.when(s + AHEAD < chunks)
+        def _():
+            gate_copy(s + AHEAD).start()
+            up_copy(s + AHEAD).start()
+
+        @pl.when(s == DOWN_START)
+        def _():
+            down_copy.start()
+
+        return carry
+
+    lax.fori_loop(1, chunks, dots, 0)
+    for copy in smalls[2:]:
+        copy.wait()
+    for side in range(2):
+        acc[side] = jnp.zeros_like(acc[side])
+
+    def gathers(s):
         for i in range(per):
             for side in range(2):
                 ag_step(s, side, i)
@@ -314,9 +320,23 @@
                 def _():
                     y_start(side)
 
+    def sums(s, carry):
+        for side in (1, 0):
+            rs_step(s, side)
+
+        @pl.when(s == chunks + 1)
+        def _():
+            down_copy.wait()
+
+        gathers(s)
         return carry
 
-    lax.fori_loop(0, STEPS, step, 0)
+    def rest(s, carry):
+        gathers(s)
+        return carry
+
+    lax.fori_loop(chunks, 2 * chunks, sums, 0)
+    lax.fori_loop(2 * chunks, STEPS, rest, 0)
 
     for side in range(2):
         @pl.when(own_side != side)
@@ -330,23 +350,18 @@
     at = 2 * z + core
     out_all[at] = spread[...].T[:8]
 
-    def out_copies(arriving):
-        made = []
-        for step in range(n):
-            for other in range(2):
-                if step or other:
-                    slot = 2 * step + other - 1
-                    source = 2 * lax.rem(z + n - step, n) + (1 - core if other else core)
-                    ref = out_all.at[source if arriving else at]
-                    made.append(pltpu.make_async_remote_copy(
-                        ref, ref, out_send.at[slot], out_recv.at[slot],
-                        device_id={"ra": lax.rem(z + step, n), "cb": mate if other else cb},
-                        device_id_type=MESH,
-                    ))
-        return made
-
-    for copy in out_copies(False):
-        copy.start()
+    for step in range(n):
+        for other in range(2):
+            if step or other:
+                pltpu.make_async_remote_copy(
+                    out_all.at[at], out_all.at[at], out_sem.at[0], out_sem.at[1],
+                    device_id={"ra": lax.rem(z + step, n), "cb": mate if other else cb},
+                    device_id_type=MESH,
+                ).start()
+    out_copies = pltpu.make_async_remote_copy(
+        out_all.at[pl.ds(0, 2 * n - 1)], out_all.at[pl.ds(0, 2 * n - 1)], out_sem.at[0], out_sem.at[1],
+        device_id={"cb": mate}, device_id_type=MESH,
+    )
     for side in range(2):
         @pl.when(own_side != side)
         def _():
@@ -360,23 +375,22 @@
         def _():
             sq_copy(side).wait_send()
 
-    def drain(j, carry):
-        @pl.when(z > 0)
-        def _():
-            rs_copy(j, 0).wait_send()
-            ag_copy(j, 1).wait_send()
-
-        @pl.when(z < n - 1)
-        def _():
-            rs_copy(j, 1).wait_send()
-            ag_copy(j, 0).wait_send()
-
-        return carry
-
-    lax.fori_loop(0, chunks, drain, 0)
-
-    for copy in out_copies(True):
-        copy.wait_recv()
+    def drain(side):
+        pltpu.make_async_remote_copy(
+            sent.at[side], got.at[side], rs_send.at[side], rs_recv.at[side, 0],
+            device_id={"ra": right if side else left}, device_id_type=MESH,
+        ).wait_send()
+        pltpu.make_async_remote_copy(
+            hidden.at[1 - side], hidden.at[1 - side], ag_send.at[1 - side], ag_recv.at[1 - side, 0],
+            device_id={"ra": right if side else left}, device_id_type=MESH,
+        ).wait_send()
+
+    for side in range(2):
+        @pl.when(z != (n - 1 if side else 0))
+        def _():
+            drain(side)
+
+    out_copies.wait_recv()
     total = out_all[0]
     for i in range(1, 2 * n):
         total = total + out_all[i]
@@ -388,8 +402,7 @@
     out_ref[:, theirs] = (mixed_got[...] * spread[:, :1] * ogain[:, theirs]).astype(jnp.bfloat16)
     for side in range(2):
         mix_copy(side).wait_send()
-    for copy in out_copies(False):
-        copy.wait_send()
+    out_copies.wait_send()
 
 
 def fused(
@@ -409,9 +422,9 @@
         out_specs=pl.BlockSpec(memory_space=pltpu.VMEM),
         scratch_shapes=[
             vmem((rows, depth), bf16), vmem((1, depth), f32),
-            vmem((blocks, depth, WIDTH), f32), vmem((units // 128, 128), f32),
-            vmem((blocks, depth, WIDTH), f32), vmem((units // 128, 128), f32),
-            vmem((blocks, WIDTH, width), f32), vmem((1, width), f32), vmem((1, width), f32),
+            vmem((chunks, depth, SUB), f32), vmem((units // 128, 128), f32),
+            vmem((chunks, depth, SUB), f32), vmem((units // 128, 128), f32),
+            vmem((units, width), f32), vmem((1, width), f32), vmem((1, width), f32),
             vmem((rows, depth), bf16), vmem((chunks, rows, 2 * SUB), f32),
             vmem((2, chunks, half, 2 * SUB), bf16), vmem((2, chunks, half, 2 * SUB), bf16),
             vmem((2, chunks, half, SUB), bf16), vmem((2, half, width), f32),
@@ -420,10 +433,9 @@
             vmem((2, half, wide), bf16), vmem((2, half, wide), bf16),
             vmem((2, half, wide), bf16), vmem((2, half, wide), bf16),
             vmem((rows, wide), f32), vmem((rows, wide), f32), vmem((2 * n, 8, 128), f32),
-            dma((6,)), dma((blocks,)), dma((blocks,)), dma((blocks,)),
-            dma((2, chunks)), dma((2, chunks)), dma((2, chunks)), dma((2, chunks)),
-            dma((2,)), dma((2,)), dma((2, 2)), dma((2, 2)), dma((2, 2)),
-            dma((2 * n - 1,)), dma((2 * n - 1,)),
+            dma((6,)), dma((AHEAD,)), dma((AHEAD,)), dma,
+            dma((2,)), dma((2, chunks)), dma((2,)), dma((2, chunks)),
+            dma((2,)), dma((2,)), dma((2, 2)), dma((2, 2)), dma((2, 2)), dma((2,)),
         ],
         compiler_params=pltpu.CompilerParams(
             collective_id=0, has_side_effects=True, vmem_limit_bytes=60 * 2**20

time: 50.3 us -> 48.3 us (0.960)
  Pallas kernels: 49.4 us -> 47.4 us
    pallas_call x1, Pallas kernels: 49.4 us -> 47.4 us  [fused(): pl.pallas_call(functools.partial(kernel, n), out_shape=pltpu.VMEM((rows,...]
where the time goes in v2:
time: 48.3 us; the launch traced here: 48.1 us
  Pallas kernels  47.4 us (98%)
  local copies, waits for them, and re-layouts  0.71 us (1%)
    pallas_call x1, Pallas kernels, fused(): pl.pallas_call(functools.partial(kernel, n), out_shape=pltpu.VMEM((rows,...  47.4 us

profile of v2, /device:TPU:0, one launch (start us, length us, event | category | flops | bytes accessed | tf_op | source)
XLA Modules:
  0.0 48.1 jit_solution(2596801897734737721)
XLA Ops:
  0.0 47.4 %fused_ffn.1 = bf16[128,1024]{1,0:T(8,128)(2,1)S(1)} custom-call(bf16[128,1024]{1,0:T(8,128)(2,1)} %tok_hbm.1, f32[1,1024]{1,0:T(1,128)} %bitcast.7, f32[1024,2816]{1,0:T(8,128)} %gate_hbm.1, f32[22,128]{1,0:T(8,128)} %bitcast.5, f32[1024,2816]{1,0:T(8,128)} %up_hbm.1, f32[22,128]{1,0:T(8,128)} %bitcast.6, f32[2816,1024]{1,0:T(8,128)} %down_hbm.1, ...), custom_call_target="tpu_custom_call" | custom-call | tf_op jit(solution)/shard_map/fused_ffn/pallas_call | solution.py:418
  47.4 0.7 %copy.11 = bf16[128,1024]{1,0:T(8,128)(2,1)} copy(bf16[128,1024]{1,0:T(8,128)(2,1)S(1)} %fused_ffn.1) | data formatting | bytes 524288

commit v3 on v2

--- a/solution.py
+++ b/solution.py
@@ -45,7 +45,7 @@
 WIDTH = 256
 SUB = 128
 AHEAD = 6
-DOWN_START = 17
+DOWN_START = 8
 RS_LAG = ((22, 12, 9, 0), (0, 7, 12, 22))
 AG_LAG = ((0, 28, 34, 44), (44, 34, 30, 0))
 OWN_SEND = (45, 40, 42, 45)
@@ -101,7 +101,9 @@
         cols = pl.ds(pl.multiple_of(j * SUB, SUB), SUB)
         return pltpu.make_async_copy(up_hbm.at[:, cols], up.at[j], up_sem.at[lax.rem(j, AHEAD)])
 
-    down_copy = pltpu.make_async_copy(down_hbm, down, down_sem)
+    def down_copy(k):
+        at = pl.ds(pl.multiple_of(k * WIDTH, WIDTH), WIDTH)
+        return pltpu.make_async_copy(down_hbm.at[at], down.at[at], down_sem)
 
     for copy in smalls[:2]:
         copy.start()
@@ -280,7 +282,7 @@
     up_copy(AHEAD).start()
 
     def dots(s, carry):
-        for side in (1, 0):
+        for side in (0, 1):
             rs_step(s, side)
         dot_step(s)
         for side in range(2):
@@ -291,9 +293,9 @@
             gate_copy(s + AHEAD).start()
             up_copy(s + AHEAD).start()
 
-        @pl.when(s == DOWN_START)
-        def _():
-            down_copy.start()
+        @pl.when((s >= DOWN_START) & (s < DOWN_START + blocks))
+        def _():
+            down_copy(s - DOWN_START).start()
 
         return carry
 
@@ -321,12 +323,12 @@
                     y_start(side)
 
     def sums(s, carry):
-        for side in (1, 0):
+        for side in (0, 1):
             rs_step(s, side)
 
         @pl.when(s == chunks + 1)
         def _():
-            down_copy.wait()
+            pltpu.make_async_copy(down_hbm, down, down_sem).wait()
 
         gathers(s)
         return carry

time: 48.3 us -> 48.1 us (level)
  no operation moved by 1% of the time
where the time goes in v3:
time: 48.1 us; the launch traced here: 47.9 us
  Pallas kernels  47.2 us (98%)
  local copies, waits for them, and re-layouts  0.71 us (1%)
    pallas_call x1, Pallas kernels, fused(): pl.pallas_call(functools.partial(kernel, n), out_shape=pltpu.VMEM((rows,...  47.2 us

profile of v3, /device:TPU:0, one launch (start us, length us, event | category | flops | bytes accessed | tf_op | source)
XLA Modules:
  0.0 47.9 jit_solution(1292511221402147360)
XLA Ops:
  0.0 47.2 %fused_ffn.1 = bf16[128,1024]{1,0:T(8,128)(2,1)S(1)} custom-call(bf16[128,1024]{1,0:T(8,128)(2,1)} %tok_hbm.1, f32[1,1024]{1,0:T(1,128)} %bitcast.7, f32[1024,2816]{1,0:T(8,128)} %gate_hbm.1, f32[22,128]{1,0:T(8,128)} %bitcast.5, f32[1024,2816]{1,0:T(8,128)} %up_hbm.1, f32[22,128]{1,0:T(8,128)} %bitcast.6, f32[2816,1024]{1,0:T(8,128)} %down_hbm.1, ...), custom_call_target="tpu_custom_call" | custom-call | tf_op jit(solution)/shard_map/fused_ffn/pallas_call | solution.py:420
  47.2 0.7 %copy.11 = bf16[128,1024]{1,0:T(8,128)(2,1)} copy(bf16[128,1024]{1,0:T(8,128)(2,1)S(1)} %fused_ffn.1) | data formatting | bytes 524288
